TPU v7x, 32 devices: a whole 2x2x4 slice. The times are simulated.
32 devices in a mesh: fs: 8 (over z, x), tp: 4 (over y, core).
Axes of the slice: x: 2, y: 2, z: 4, core: 2. Of those that a mesh axis runs over, the one named last changes fastest.
Arguments:
- tokens: bfloat16 [6144, 2048], P('fs', 'tp'), may hold values from -6 to 6
- mix_gain: float32 [2048], replicated, may hold values from 0.1 to 1.9
- outer_gate: bfloat16 [2048, 2048], P('fs', 'tp'), may hold values from -0.125 to 0.125
- inner_gate: bfloat16 [2048, 2048], P('fs', 'tp'), may hold values from -0.125 to 0.125
- signal_in: bfloat16 [2048, 2048], P('fs', 'tp'), may hold values from -0.125 to 0.125
- mix_taps: float32 [3, 2048], P(None, 'tp'), may hold values from -3 to 3
- mix_bias: float32 [2048], P('tp'), may hold values from -3 to 3
- mix_out: bfloat16 [2048, 2048], P('tp', 'fs'), may hold values from -0.1875 to 0.1875
- ffn_gain: float32 [2048], replicated, may hold values from 0.1 to 1.9
- up_gate: bfloat16 [2048, 5632], P('fs', 'tp'), may hold values from -0.125 to 0.125
- up_value: bfloat16 [2048, 5632], P('fs', 'tp'), may hold values from -0.125 to 0.125
- ffn_taps: float32 [2, 3, 5632], P(None, None, 'tp'), may hold values from -3 to 3
- ffn_bias: float32 [2, 5632], P(None, 'tp'), may hold values from -3 to 3
- down_proj: bfloat16 [5632, 2048], P('tp', 'fs'), may hold values from -0.109375 to 0.109375
Outputs:
- layer_out: bfloat16 [6144, 2048], P('fs', 'tp')
All inputs are finite; a program needn't handle non-finite values.
Results may differ from a plain program's by a relative error of at most 0.023.
Values may be sent and summed in bfloat16 or wider, within the bound.
A program may use at most 64 MiB of HBM per device.

v0:
```python
import jax
import jax.numpy as jnp
from jax import lax
from jax.sharding import PartitionSpec as P

EPS = 1e-06


def gather_rows(column_part):
    return lax.all_gather(column_part, "tp", axis=1, tiled=True)


def rms_rows(values, gain):
    floats = values.astype(jnp.float32)
    scaled = floats * lax.rsqrt(jnp.mean(floats * floats, axis=-1, keepdims=True) + EPS) * gain
    return scaled.astype(jnp.bfloat16)


def causal_taps(signal, taps, bias):
    first = jnp.pad(signal, ((1, 0), (0, 0)))[:-1]
    second = jnp.pad(signal, ((2, 0), (0, 0)))[:-2]
    return taps[2] * signal + taps[1] * first + taps[0] * second + bias


def project_out(active, weight):
    return jnp.dot(
        active, lax.all_gather(weight, "fs", axis=1, tiled=True), preferred_element_type=jnp.float32
    )


def share_cols(term):
    return lax.psum_scatter(
        term.astype(jnp.bfloat16), "tp", scatter_dimension=1, tiled=True
    ).astype(jnp.float32)


def fold_products(normed, pieces):
    return tuple((jnp.dot(normed, piece, preferred_element_type=jnp.float32) for piece in pieces))


def on_device(
    tokens,
    mix_gain,
    outer_gate,
    inner_gate,
    signal_in,
    mix_taps,
    mix_bias,
    mix_out,
    ffn_gain,
    up_gate,
    up_value,
    ffn_taps,
    ffn_bias,
    down_proj,
):
    full_rows = gather_rows(tokens)
    normed = rms_rows(full_rows, mix_gain)
    outer, inner, signal = fold_products(
        normed,
        (
            lax.all_gather(outer_gate, "fs", axis=0, tiled=True),
            lax.all_gather(inner_gate, "fs", axis=0, tiled=True),
            lax.all_gather(signal_in, "fs", axis=0, tiled=True),
        ),
    )
    outer = outer.astype(jnp.bfloat16).astype(jnp.float32)
    inner = inner.astype(jnp.bfloat16).astype(jnp.float32)
    signal = signal.astype(jnp.bfloat16).astype(jnp.float32)
    gated = (outer * causal_taps(inner * signal, mix_taps, mix_bias)).astype(jnp.bfloat16)
    mix_term = project_out(gated, mix_out)
    total = lax.psum(mix_term.astype(jnp.bfloat16), "tp").astype(jnp.float32)
    state_rows = (full_rows.astype(jnp.float32) + total).astype(jnp.bfloat16)
    own_width = tokens.shape[1]
    state_cols = lax.dynamic_slice_in_dim(
        state_rows, lax.axis_index("tp") * own_width, own_width, 1
    )
    normed_two = rms_rows(state_rows, ffn_gain)
    gate_pre, value_pre = fold_products(
        normed_two,
        (
            lax.all_gather(up_gate, "fs", axis=0, tiled=True),
            lax.all_gather(up_value, "fs", axis=0, tiled=True),
        ),
    )
    gate_pre = gate_pre.astype(jnp.bfloat16).astype(jnp.float32)
    value_pre = value_pre.astype(jnp.bfloat16).astype(jnp.float32)
    gate_conv = causal_taps(gate_pre, ffn_taps[0], ffn_bias[0])
    value_conv = causal_taps(value_pre, ffn_taps[1], ffn_bias[1])
    active = (jax.nn.silu(gate_conv) * value_conv).astype(jnp.bfloat16)
    fed = share_cols(project_out(active, down_proj))
    return (state_cols.astype(jnp.float32) + fed).astype(jnp.bfloat16)


def solution(mesh):
    return jax.shard_map(
        on_device,
        mesh=mesh,
        in_specs=(
            P("fs", "tp"),
            P(),
            P("fs", "tp"),
            P("fs", "tp"),
            P("fs", "tp"),
            P(None, "tp"),
            P("tp"),
            P("tp", "fs"),
            P(),
            P("fs", "tp"),
            P("fs", "tp"),
            P(None, None, "tp"),
            P(None, "tp"),
            P("tp", "fs"),
        ),
        out_specs=P("fs", "tp"),
        check_vma=False,
    )
```

profile of v0, /device:TPU:0, one launch (start us, length us, event | category | flops | bytes accessed | tf_op | source)
XLA Modules:
  0.0 661.6 jit_solution(12850123680895059414)
XLA Ops:
  6.5 0.7 all-gather.9.cloned.1.call-update
  7.3 0.7 all-gather.15.cloned.1.call-update
  8.1 0.7 all-gather.13.cloned.1.call-update
  8.8 0.5 all-gather.11.cloned.1.call-update
  9.4 0.5 all-gather.17.cloned.1.call-update
  9.9 0.0 all-reduce.8.cloned.1.call-start
  10.0 0.8 fusion.39
  10.8 29.4 %all-gather.9.cloned.1.call-done = bf16[768,2048]{1,0:T(8,128)(2,1)} async-done(((bf16[768,512]{1,0:T(8,128)(2,1)}), bf16[768,2048]{1,0:T(8,128)(2,1)}) %all-gather.9.cloned.1.call-update) | async-done | bytes 3145744 | tf_op jit(solution)/shard_map/all_gather | solution.py:10
  40.2 2.6 fusion.3
  42.8 48.6 %all-gather.15.cloned.1.call-done = bf16[2048,512]{1,0:T(8,128)(2,1)} async-done(((bf16[256,512]{1,0:T(8,128)(2,1)}), bf16[2048,512]{1,0:T(8,128)(2,1)}) %all-gather.15.cloned.1.call-update) | async-done | bytes 2097168 | tf_op jit(solution)/shard_map/all_gather | solution.py:64
  91.4 5.3 convolution_convert_fusion.4
  96.7 44.5 %all-gather.13.cloned.1.call-done = bf16[2048,512]{1,0:T(8,128)(2,1)} async-done(((bf16[256,512]{1,0:T(8,128)(2,1)}), bf16[2048,512]{1,0:T(8,128)(2,1)}) %all-gather.13.cloned.1.call-update) | async-done | bytes 2097168 | tf_op jit(solution)/shard_map/all_gather | solution.py:63
  141.2 4.8 convert_multiply_fusion.4
  146.0 44.9 %all-gather.11.cloned.1.call-done = bf16[2048,512]{1,0:T(8,128)(2,1)} async-done(((bf16[256,512]{1,0:T(8,128)(2,1)}), bf16[2048,512]{1,0:T(8,128)(2,1)}) %all-gather.11.cloned.1.call-update) | async-done | bytes 2097168 | tf_op jit(solution)/shard_map/all_gather | solution.py:62
  190.8 50.8 %all-gather.17.cloned.1.call-done = bf16[512,2048]{1,0:T(8,128)(2,1)} async-done(((bf16[512,256]{1,0:T(8,128)(2,1)}), bf16[512,2048]{1,0:T(8,128)(2,1)}) %all-gather.17.cloned.1.call-update) | async-done | bytes 2097168 | tf_op jit(solution)/shard_map/all_gather | solution.py:27
  241.6 9.3 %convolution_convert_fusion = bf16[768,2048]{1,0:T(8,128)(2,1)} fusion(bf16[512,2048]{1,0:T(8,128)(2,1)} %all-gather.17.cloned.1.call-done, f32[768,512]{1,0:T(8,128)} %convert_multiply_fusion.4, bf16[2048,512]{1,0:T(8,128)(2,1)} %all-gather.11.cloned.1.call-done, f32[512]{0:T(512)S(1)} %copy-done.6, f32[512]{0:T(512)S(1)} %bitcast.11, ...), kind=kOutput, calls=%fused_computation.28 | convolution fusion | flops 3233021952 | bytes 12078080 | tf_op jit(solution)/shard_map/dot_general | solution.py:26
  250.9 0.0 all-gather.19.cloned.1.call-start
  251.0 0.7 all-gather.19.cloned.1.call-update
  251.7 0.7 all-gather.21.cloned.1.call-update
  252.5 0.7 all-gather.23.cloned.1.call-update
  253.1 0.2 reduce-scatter.2.cloned.1.call-start
  253.4 0.1 slice_reduce_fusion.7
  253.5 64.2 %all-reduce.8.cloned.1.call-done = bf16[768,2048]{1,0:T(8,128)(2,1)} async-done(((bf16[768,2048]{1,0:T(8,128)(2,1)}), bf16[768,2048]{1,0:T(8,128)(2,1)}) %all-reduce.8.cloned.1.call-update) | async-done | bytes 3145744 | tf_op jit(solution)/shard_map/psum | solution.py:72
  317.7 5.1 fusion
  322.8 89.5 %all-gather.19.cloned.1.call-done = bf16[2048,1408]{1,0:T(8,128)(2,1)} async-done(((bf16[256,1408]{1,0:T(8,128)(2,1)}), bf16[2048,1408]{1,0:T(8,128)(2,1)}) %all-gather.19.cloned.1.call-update) | async-done | bytes 5767184 | tf_op jit(solution)/shard_map/all_gather | solution.py:82
  412.3 10.0 %fusion.20 = f32[768,1408]{1,0:T(8,128)} fusion(bf16[2048,1408]{1,0:T(8,128)(2,1)} %all-gather.19.cloned.1.call-done, bf16[768,2048]{1,0:T(8,128)(2,1)} %get-tuple-element.14, f32[2048]{0:T(1024)S(1)} %copy-done.5, f32[768]{0:T(1024)S(1)} %add_rsqrt_fusion), kind=kOutput, calls=%fused_computation.33 | convolution fusion | flops 4437639168 | bytes 13249536 | tf_op jit(solution)/shard_map/dot_general | solution.py:38
  422.3 82.7 %all-gather.21.cloned.1.call-done = bf16[2048,1408]{1,0:T(8,128)(2,1)} async-done(((bf16[256,1408]{1,0:T(8,128)(2,1)}), bf16[2048,1408]{1,0:T(8,128)(2,1)}) %all-gather.21.cloned.1.call-update) | async-done | bytes 5767184 | tf_op jit(solution)/shard_map/all_gather | solution.py:83
  505.0 9.4 %fusion.19 = f32[768,1408]{1,0:T(8,128)} fusion(bf16[2048,1408]{1,0:T(8,128)(2,1)} %all-gather.21.cloned.1.call-done, bf16[768,2048]{1,0:T(8,128)(2,1)S(1)} %copy-done.1, f32[2048]{0:T(1024)S(1)} %copy-done.5, f32[768]{0:T(1024)S(1)} %add_rsqrt_fusion), kind=kOutput, calls=%fused_computation.31 | convolution fusion | flops 4437639168 | bytes 13249536 | tf_op jit(solution)/shard_map/dot_general | solution.py:38
  514.4 84.0 %all-gather.23.cloned.1.call-done = bf16[1408,2048]{1,0:T(8,128)(2,1)} async-done(((bf16[1408,256]{1,0:T(8,128)(2,1)}), bf16[1408,2048]{1,0:T(8,128)(2,1)}) %all-gather.23.cloned.1.call-update) | async-done | bytes 5767184 | tf_op jit(solution)/shard_map/all_gather | solution.py:27
  598.4 18.0 %convolution_convert_fusion.1 = bf16[768,2048]{1,0:T(8,128)(2,1)} fusion(bf16[1408,2048]{1,0:T(8,128)(2,1)} %all-gather.23.cloned.1.call-done, f32[768,1408]{1,0:T(8,128)} %fusion.19, f32[768,1408]{1,0:T(8,128)} %fusion.20, f32[1408]{0:T(1024)S(1)} %get-tuple-element.12, f32[1408]{0:T(1024)S(1)} %get-tuple-element.9, f32[1408]{0:T(1024)S(1)} %get-tuple-element.10, ...), kind=kOutput, calls=%fused_computation.29 | convolution fusion | flops 4450222080 | bytes 17608704 | tf_op jit(solution)/shard_map/dot_general | solution.py:26
  616.4 36.1 %reduce-scatter.2.cloned.1.call-done = bf16[768,512]{1,0:T(8,128)(2,1)} async-done(((bf16[768,2048]{1,0:T(8,128)(2,1)}), bf16[768,512]{1,0:T(8,128)(2,1)}) %reduce-scatter.2.cloned.1.call-update) | async-done | bytes 786448 | tf_op jit(solution)/shard_map/reduce_scatter | solution.py:32
  652.5 2.3 add_convert_fusion
  (26 shorter events, 0.3 us)
Async XLA Ops:
  6.5 84.9 %copy-start.4 = (f32[2048]{0:T(1024)S(1)}, f32[2048]{0:T(1024)}, u32[]{:S(2)}) copy-start(f32[2048]{0:T(1024)} %param.15) | copy-start | bytes 24580
  6.5 33.6 %all-gather.9.cloned.1.call-start = ((), (), s32[]{:S(2)}) async-start(), calls=%async_computation.1 | async-start | bytes 3932160 | tf_op jit(solution)/shard_map/all_gather | solution.py:10
  7.3 84.1 %all-gather.15.cloned.1.call-start = ((), (), s32[]{:S(2)}) async-start(), calls=%async_computation.4 | async-start | bytes 2359296 | tf_op jit(solution)/shard_map/all_gather | solution.py:64
  8.0 133.2 %all-gather.13.cloned.1.call-start = ((), (), s32[]{:S(2)}) async-start(), calls=%async_computation.3 | async-start | bytes 2359296 | tf_op jit(solution)/shard_map/all_gather | solution.py:63
  8.7 182.1 %all-gather.11.cloned.1.call-start = ((), (), s32[]{:S(2)}) async-start(), calls=%async_computation.2 | async-start | bytes 2359296 | tf_op jit(solution)/shard_map/all_gather | solution.py:62
  9.3 232.3 %all-gather.17.cloned.1.call-start = ((), (), s32[]{:S(2)}) async-start(), calls=%async_computation.5 | async-start | bytes 2359296 | tf_op jit(solution)/shard_map/all_gather | solution.py:27
  9.9 307.8 %all-reduce.8.cloned.1.call-start = ((), (), s32[]{:S(2)}) async-start(), calls=%async_computation.6 | async-start | bytes 6291456 | tf_op jit(solution)/shard_map/psum | solution.py:72
  42.7 98.4 %copy-start = (bf16[768,2048]{1,0:T(8,128)(2,1)S(1)}, bf16[768,2048]{1,0:T(8,128)(2,1)}, u32[]{:S(2)}) copy-start(bf16[768,2048]{1,0:T(8,128)(2,1)} %all-gather.9.cloned.1.call-done) | copy-start | bytes 9437188
  96.7 145.0 %copy-start.6 = (f32[512]{0:T(512)S(1)}, f32[512]{0:T(512)}, u32[]{:S(2)}) copy-start(f32[512]{0:T(512)} %param.20) | copy-start | bytes 6148
  250.9 2.5 copy-start.3
  250.9 2.5 copy-start.2
  250.9 161.4 %all-gather.19.cloned.1.call-start = ((), (), s32[]{:S(2)}) async-start(), calls=%async_computation.7 | async-start | bytes 6488064 | tf_op jit(solution)/shard_map/all_gather | solution.py:82
  251.7 253.4 %all-gather.21.cloned.1.call-start = ((), (), s32[]{:S(2)}) async-start(), calls=%async_computation.8 | async-start | bytes 6488064 | tf_op jit(solution)/shard_map/all_gather | solution.py:83
  252.4 346.0 %all-gather.23.cloned.1.call-start = ((), (), s32[]{:S(2)}) async-start(), calls=%async_computation.9 | async-start | bytes 6488064 | tf_op jit(solution)/shard_map/all_gather | solution.py:27
  253.1 399.4 %reduce-scatter.2.cloned.1.call-start = ((), (), s32[]{:S(2)}) async-start(), calls=%async_computation.10 | async-start | bytes 3932160 | tf_op jit(solution)/shard_map/reduce_scatter | solution.py:32
  253.5 158.8 %copy-start.5 = (f32[2048]{0:T(1024)S(1)}, f32[2048]{0:T(1024)}, u32[]{:S(2)}) copy-start(f32[2048]{0:T(1024)} %param.22) | copy-start | bytes 24580
  412.3 92.7 %copy-start.1 = (bf16[768,2048]{1,0:T(8,128)(2,1)S(1)}, bf16[768,2048]{1,0:T(8,128)(2,1)}, u32[]{:S(2)}) copy-start(bf16[768,2048]{1,0:T(8,128)(2,1)} %get-tuple-element.14) | copy-start | bytes 9437188
Sparse Core Ops, SparseCore 0:
  8.9 31.2 all-gather.8
  42.3 49.0 all-gather.14
  93.5 47.6 all-gather.12
  143.2 47.6 all-gather.10
  192.7 48.8 all-gather.16
  251.0 66.6 all-reduce.7
  319.9 92.3 all-gather.18
  414.5 90.4 all-gather.20
  507.1 91.3 all-gather.22
  616.5 35.9 reduce-scatter.1
where the time goes:
time: 662 us
  waiting for transfers between devices  580 us (88%)
  matrix products  56.6 us (9%)
  between operations  13.6 us (2%)
  other arithmetic  9.97 us (2%)
    all_gather x2, waiting for transfers between devices, project_out(): lax.all_gather(weight, 'fs', axis=1, tiled=True)  135 us
    all_gather x1, waiting for transfers between devices, on_device(): lax.all_gather(up_gate, 'fs', axis=0, tiled=True)  89.5 us
    all_gather x1, waiting for transfers between devices, on_device(): lax.all_gather(up_value, 'fs', axis=0, tiled=True)  82.7 us
    psum x1, waiting for transfers between devices, on_device(): total = lax.psum(mix_term.astype(jnp.bfloat16), 'tp').astype(jnp.float32)  64.2 us
    all_gather x1, waiting for transfers between devices, on_device(): lax.all_gather(signal_in, 'fs', axis=0, tiled=True)  48.6 us
    all_gather x1, waiting for transfers between devices, on_device(): lax.all_gather(outer_gate, 'fs', axis=0, tiled=True)  44.9 us
    all_gather x1, waiting for transfers between devices, on_device(): lax.all_gather(inner_gate, 'fs', axis=0, tiled=True)  44.5 us
    reduce_scatter x1, waiting for transfers between devices, share_cols(): lax.psum_scatter(term.astype(jnp.bfloat16), 'tp', scatter_dimension=1, ti...  36.1 us
  transfers between devices with their start and end apart: 10, of which 10 were waited for; matrix products, arithmetic and copies ran while one was open for 6% of the time, Pallas kernels for 0%

commit v1 on v0

v1 whole, which is shorter than its diff:
```python
import functools

import jax
import jax.numpy as jnp
from jax import lax
from jax.experimental import pallas as pl
from jax.experimental.pallas import tpu as pltpu
from jax.sharding import PartitionSpec as P

EPS = 1e-06
F32, BF16 = jnp.float32, jnp.bfloat16
MESH = pl.DeviceIdType.MESH
UP, DOWN, RIGHT, LEFT = range(4)


def grid_of(n_fs):
    nx = 1
    while nx * nx * 4 <= n_fs:
        nx *= 2
    return n_fs // nx, nx


def tiles(extent, width, body):
    whole = extent // width
    if whole:
        @pl.loop(0, whole)
        def _(i):
            body(pl.multiple_of(i * width, width), width)
    if extent % width:
        body(whole * width, extent % width)


def causal(v, taps, bias):
    row = lax.broadcasted_iota(jnp.int32, v.shape, 0)
    first = jnp.where(row < 1, 0.0, pltpu.roll(v, 1, axis=0))
    second = jnp.where(row < 2, 0.0, pltpu.roll(v, 2, axis=0))
    return taps[2] * v + taps[1] * first + taps[0] * second + bias


def kernel(
    n_fs, n_tp, tok_in, og, ig, si, mo, ug, uv, dp,
    mix_gain, ffn_gain, mix_taps, mix_bias, ffn_taps, ffn_bias,
    out,
    w0, w1, w2, w3, w4, w5, w6,
    tok, normed, state, outer, inner, signal, gate, value,
    part1, rs1, part2, rs2,
    load_sem, send_sem, recv_sem,
    tok_send, tok_recv, st_send, st_recv, p1_send, p1_recv, p2_send, p2_recv,
):
    nz, nx = grid_of(n_fs)
    fs, tp = lax.axis_index("fs"), lax.axis_index("tp")
    z, x = fs // nx, fs % nx
    bufs = (w0, w1, w2, w3, w4, w5, w6)
    sources = (og, ig, si, mo, ug, uv, dp)
    rows, own = tok.shape[1], tok.shape[2]
    per = n_fs // n_tp
    wide = part1.shape[2]

    ways = (
        (z < nz - 1, fs + nx),
        (z > 0, fs - nx),
        (x < nx - 1, fs + 1),
        (x > 0, fs - 1),
    )
    barrier = pltpu.get_barrier_semaphore()
    expected = n_tp - 1
    for there, peer in ways:
        expected = expected + jnp.where(there, 1, 0)

        @pl.when(there)
        def _(peer=peer):
            pl.semaphore_signal(barrier, inc=1, device_id={"fs": peer}, device_id_type=MESH)
    peers = [(tp + r) % n_tp for r in range(1, n_tp)]
    for peer in peers:
        pl.semaphore_signal(barrier, inc=1, device_id={"tp": peer}, device_id_type=MESH)

    loads = [pltpu.make_async_copy(s, b.at[fs], load_sem.at[i]) for i, (s, b) in enumerate(zip(sources, bufs))]
    loads.append(pltpu.make_async_copy(tok_in, tok.at[tp], load_sem.at[7]))
    for c in loads:
        c.start()
    pl.semaphore_wait(barrier, expected)

    def cut(w):
        r = bufs[w].shape[1]
        a = max(16, (r * 13 // 16) // 16 * 16)
        return ((0, a), (a, r - a))

    def piece(w, k, block, way):
        start, size = cut(w)[k]
        ref = bufs[w].at[block, pl.ds(start, size)]
        return pltpu.make_async_remote_copy(
            src_ref=ref, dst_ref=ref,
            send_sem=send_sem.at[w, k, block, way], recv_sem=recv_sem.at[w, k, block],
            device_id={"fs": ways[way][1]}, device_id_type=MESH,
        )

    def arrive(w, k, block):
        piece(w, k, block, UP).wait_recv()

    def go(w, k, block, way, cond, sending):
        @pl.when(jnp.logical_and(cond, ways[way][0]))
        def _():
            c = piece(w, k, block, way)
            if sending:
                c.start()
            else:
                c.wait_send()

    yes = z >= 0

    def along_z(w, i, sending, block_ready=None):
        half = (i + 1) // 2
        off = jnp.where(i % 2 == 1, -half, half)
        z0 = z + off
        valid = jnp.logical_and(z0 >= 0, z0 < nz)
        away = off != 0

        @pl.when(valid)
        def _():
            mine = z0 * nx + x

            def both(k, block):
                go(w, k, block, UP, z0 <= z, sending)
                go(w, k, block, DOWN, z0 >= z, sending)

            if sending:
                @pl.when(away)
                def _():
                    arrive(w, 0, mine)
            both(0, mine)
            go(w, 0, mine, RIGHT, yes, sending)
            go(w, 0, mine, LEFT, yes, sending)
            for x0 in range(nx):
                block = z0 * nx + x0
                if sending:
                    @pl.when(jnp.logical_or(away, x != x0))
                    def _():
                        arrive(w, 1, block)
                level = jnp.logical_not(away)
                go(w, 1, block, RIGHT, jnp.logical_and(level, x0 <= x), sending)
                go(w, 1, block, LEFT, jnp.logical_and(level, x0 >= x), sending)
                both(1, block)
            if block_ready is not None:
                block_ready(mine)

    def along_x(w, i, sending, block_ready=None):
        half = (i + 1) // 2
        z0 = z + jnp.where(i % 2 == 1, -half, half)

        @pl.when(jnp.logical_and(z0 >= 0, z0 < nz))
        def _():
            for dist in range(1, nx):
                for sign in (-1, 1):
                    x0 = x + sign * dist

                    @pl.when(jnp.logical_and(x0 >= 0, x0 < nx))
                    def _(sign=sign, x0=x0):
                        block = z0 * nx + x0
                        if sending:
                            arrive(w, 0, block)
                        go(w, 0, block, RIGHT if sign < 0 else LEFT, yes, sending)
            if block_ready is not None:
                @pl.loop(1, nx)
                def _(j):
                    block_ready(z0 * nx + (x + j) % nx)

    steps = 2 * nz - 1

    def pump(w, lo=1, hi=None, block_ready=None):
        last = steps + 1 if hi is None else hi

        @pl.loop(lo, last)
        def _(i):
            @pl.when(i < steps)
            def _():
                along_z(w, i, True, block_ready)
            along_x(w, i - 1, True, block_ready)

    def begin(w):
        loads[w].wait()
        along_z(w, 0, True)

    def to_owner(part, rs, send, recv, block):
        owner, k = block // per, block % per
        return owner, pltpu.make_async_remote_copy(
            src_ref=part.at[block], dst_ref=rs.at[tp, k],
            send_sem=send.at[block], recv_sem=recv.at[tp, k],
            device_id={"tp": owner}, device_id_type=MESH,
        )

    def from_peer(rs, recv, src, k):
        ref = rs.at[src, k]
        pltpu.make_async_remote_copy(
            src_ref=ref, dst_ref=ref, send_sem=p1_send.at[0], recv_sem=recv.at[src, k],
            device_id={"tp": src}, device_id_type=MESH,
        ).wait_recv()

    def spread(buf, send, recv):
        return [
            pltpu.make_async_remote_copy(
                src_ref=buf.at[tp], dst_ref=buf.at[tp], send_sem=send.at[r], recv_sem=recv.at[tp],
                device_id={"tp": peer}, device_id_type=MESH,
            )
            for r, peer in enumerate(peers)
        ]

    def collect(buf, send, recv):
        for peer in peers:
            pltpu.make_async_remote_copy(
                src_ref=buf.at[peer], dst_ref=buf.at[peer], send_sem=send.at[0], recv_sem=recv.at[peer],
                device_id={"tp": peer}, device_id_type=MESH,
            ).wait_recv()

    def norm(buf, gain):
        step = 64

        @pl.loop(0, rows // step)
        def _(m):
            at = pl.ds(pl.multiple_of(m * step, step), step)
            total = jnp.zeros((step, 1), F32)
            for t in range(n_tp):
                v = buf[t, at, :].astype(F32)
                total = total + jnp.sum(v * v, axis=-1, keepdims=True)
            scale = lax.rsqrt(total / (n_tp * own) + EPS)
            for t in range(n_tp):
                cols = slice(t * own, (t + 1) * own)
                v = buf[t, at, :].astype(F32)
                normed[at, cols] = (v * scale * gain[:, cols]).astype(BF16)

    mt = 256 if rows % 256 == 0 else rows

    def project(w, dst):
        n, r, c = bufs[w].shape

        def column(start, size):
            @pl.loop(0, rows // mt)
            def _(m):
                at = pl.ds(pl.multiple_of(m * mt, mt), mt)
                weight = bufs[w][:, :, pl.ds(start, size)].reshape(n * r, size)
                dst[at, pl.ds(start, size)] = jnp.dot(
                    normed[at, :], weight, preferred_element_type=F32
                ).astype(BF16)
        tiles(c, 256, column)

    def out_block(w, act, part, rs, send, recv, block):
        @pl.loop(0, rows // mt)
        def _(m):
            at = pl.ds(pl.multiple_of(m * mt, mt), mt)
            part[block, at, :] = jnp.dot(
                act[at, :], bufs[w][block], preferred_element_type=F32
            ).astype(BF16)
        owner, c = to_owner(part, rs, send, recv, block)

        @pl.when(owner != tp)
        def _():
            c.start()

    def add_up(base, part, rs, recv, dst):
        for peer in peers:
            for k in range(per):
                from_peer(rs, recv, peer, k)
        step = 128

        @pl.loop(0, rows // step)
        def _(m):
            at = pl.ds(pl.multiple_of(m * step, step), step)
            for k in range(per):
                cols = slice(k * wide, (k + 1) * wide)
                total = part[tp * per + k, at, :].astype(F32)
                for peer in peers:
                    total = total + rs[peer, k, at, :].astype(F32)
                dst[at, cols] = (base[at, cols].astype(F32) + total).astype(BF16)

    loads[7].wait()
    begin(0)
    begin(1)
    tok_copies = spread(tok, tok_send, tok_recv)
    for c in tok_copies:
        c.start()
    pump(0)
    begin(2)
    pump(1)
    begin(3)
    collect(tok, tok_send, tok_recv)
    norm(tok, mix_gain)
    pump(2, 1, 4)
    project(0, outer)
    pump(2, 4)
    begin(4)
    project(1, inner)
    pump(3, 1, 4)
    project(2, signal)

    def mixer(start, size):
        cols = pl.ds(start, size)
        taps = [mix_taps[j:j + 1, cols] for j in range(3)]
        v = inner[:, cols].astype(F32) * signal[:, cols].astype(F32)
        outer[:, cols] = (outer[:, cols].astype(F32) * causal(v, taps, mix_bias[:, cols])).astype(BF16)
    tiles(outer.shape[1], 128, mixer)
    pump(3, 4)
    begin(5)

    @pl.loop(0, n_fs)
    def _(block):
        out_block(3, outer, part1, rs1, p1_send, p1_recv, block)
    pump(4, 1, 4)
    add_up(tok.at[tp], part1, rs1, p1_recv, state.at[tp])
    st_copies = spread(state, st_send, st_recv)
    for c in st_copies:
        c.start()
    pump(4, 4)
    begin(6)
    pump(5, 1, 4)
    collect(state, st_send, st_recv)
    norm(state, ffn_gain)
    project(4, gate)
    pump(5, 4)

    pump(6, 1, 3)
    project(5, value)

    def feed(start, size):
        cols = pl.ds(start, size)
        g = causal(gate[:, cols].astype(F32), [ffn_taps[j:j + 1, cols] for j in range(3)], ffn_bias[0:1, cols])
        v = causal(value[:, cols].astype(F32), [ffn_taps[j:j + 1, cols] for j in range(3, 6)], ffn_bias[1:2, cols])
        gate[:, cols] = (g / (1.0 + jnp.exp(-g)) * v).astype(BF16)
    tiles(gate.shape[1], 128, feed)

    @pl.loop(0, steps + 1)
    def _(i):
        def block_out(block):
            out_block(6, gate, part2, rs2, p2_send, p2_recv, block)

        half = (i + 1) // 2
        z0 = z + jnp.where(i % 2 == 1, -half, half)
        before = i // 2
        z1 = z + jnp.where(i % 2 == 0, -before, before)

        @pl.when(jnp.logical_and(i >= 3, i < steps))
        def _():
            along_z(6, i, True)

        @pl.when(i >= 3)
        def _():
            along_x(6, i - 1, True)

        @pl.loop(0, nx)
        def _(j):
            z_of = jnp.where(j == 0, z0, z1)
            good = jnp.logical_and(z_of >= 0, z_of < nz)
            good = jnp.logical_and(good, jnp.where(j == 0, i < steps, i >= 1))

            @pl.when(good)
            def _():
                block_out(z_of * nx + (x + j) % nx)

    add_up(state.at[tp], part2, rs2, p2_recv, out)

    for c in tok_copies + st_copies:
        c.wait_send()
    for part, rs, send, recv in ((part1, rs1, p1_send, p1_recv), (part2, rs2, p2_send, p2_recv)):
        @pl.loop(0, n_fs)
        def _(block):
            owner, c = to_owner(part, rs, send, recv, block)

            @pl.when(owner != tp)
            def _():
                c.wait_send()
    for w in range(7):
        @pl.loop(0, steps)
        def _(i):
            along_z(w, i, False)
            along_x(w, i, False)


def solution(mesh):
    n_fs, n_tp = mesh.shape["fs"], mesh.shape["tp"]

    def on_device(
        tokens, mix_gain, outer_gate, inner_gate, signal_in, mix_taps, mix_bias, mix_out,
        ffn_gain, up_gate, up_value, ffn_taps, ffn_bias, down_proj,
    ):
        rows, own = tokens.shape
        weights = (outer_gate, inner_gate, signal_in, mix_out, up_gate, up_value, down_proj)
        chan, hidden = outer_gate.shape[1], up_gate.shape[1]
        wide = mix_out.shape[1]
        model = own * n_tp
        hbm = pl.BlockSpec(memory_space=pl.ANY)
        vmem = pl.BlockSpec(memory_space=pltpu.VMEM)
        dma = pltpu.SemaphoreType.DMA
        per = n_fs // n_tp
        return pl.pallas_call(
            functools.partial(kernel, n_fs, n_tp),
            out_shape=jax.ShapeDtypeStruct(tokens.shape, BF16),
            in_specs=[hbm] * 8 + [vmem] * 6,
            out_specs=vmem,
            scratch_shapes=[pltpu.VMEM((n_fs, *w.shape), BF16) for w in weights]
            + [
                pltpu.VMEM((n_tp, rows, own), BF16),
                pltpu.VMEM((rows, model), BF16),
                pltpu.VMEM((n_tp, rows, own), BF16),
                pltpu.VMEM((rows, chan), BF16),
                pltpu.VMEM((rows, chan), BF16),
                pltpu.VMEM((rows, chan), BF16),
                pltpu.VMEM((rows, hidden), BF16),
                pltpu.VMEM((rows, hidden), BF16),
                pltpu.VMEM((n_fs, rows, wide), BF16),
                pltpu.VMEM((n_tp, per, rows, wide), BF16),
                pltpu.VMEM((n_fs, rows, wide), BF16),
                pltpu.VMEM((n_tp, per, rows, wide), BF16),
                dma((8,)),
                dma((7, 2, n_fs, 4)),
                dma((7, 2, n_fs)),
                dma((n_tp,)), dma((n_tp,)),
                dma((n_tp,)), dma((n_tp,)),
                dma((n_fs,)), dma((n_tp, per)),
                dma((n_fs,)), dma((n_tp, per)),
            ],
            compiler_params=pltpu.CompilerParams(
                collective_id=0, has_side_effects=True, vmem_limit_bytes=67043328
            ),
        )(
            tokens, *weights, mix_gain[None], ffn_gain[None], mix_taps, mix_bias[None],
            ffn_taps.reshape(6, hidden), ffn_bias,
        )

    return jax.shard_map(
        on_device,
        mesh=mesh,
        in_specs=(
            P("fs", "tp"), P(), P("fs", "tp"), P("fs", "tp"), P("fs", "tp"), P(None, "tp"), P("tp"),
            P("tp", "fs"), P(), P("fs", "tp"), P("fs", "tp"), P(None, None, "tp"), P(None, "tp"),
            P("tp", "fs"),
        ),
        out_specs=P("fs", "tp"),
        check_vma=False,
    )
```

time: 662 us -> 349 us (0.53)
  waiting for transfers between devices: 580 us -> 0 us
  Pallas kernels: 0 us -> 345 us
  matrix products: 56.6 us -> 0 us
  between operations: 13.6 us -> 0.01 us
  other arithmetic: 9.97 us -> 0 us
    all_gather x8 -> x0, waiting for transfers between devices: 474 us -> none  [the longest x2 135 us: project_out(): lax.all_gather(weight, 'fs', axis=1, tiled=True)]
    pallas_call x0 -> x1, Pallas kernels: none -> 345 us  [on_device(): pl.pallas_call(functools.partial(kernel, n_fs, n_tp), out_shape=jax.Shape...]
    psum x1 -> x0, waiting for transfers between devices: 64.2 us -> none  [on_device(): total = lax.psum(mix_term.astype(jnp.bfloat16), 'tp').astype(jnp.float32)]
    dot_general x6 -> x0, matrix products: 56.6 us -> none  [the longest x4 29.4 us: fold_products(): jnp.dot(normed, piece, preferred_element_type=jnp.float32)]
    reduce_scatter x1 -> x0, waiting for transfers between devices: 36.1 us -> none  [share_cols(): lax.psum_scatter(term.astype(jnp.bfloat16), 'tp', scatter_dimension=1, ti...]
    reduce_sum x2 -> x0, other arithmetic: 7.67 us -> none  [rms_rows(): jnp.mean(floats * floats, axis=-1, keepdims=True) + EPS]
  transfers between devices with their start and end apart: 10 -> 0, of which waited for: 10 -> 0; matrix products, arithmetic and copies ran while one was open for 6% -> 0% of each run, Pallas kernels for 0% -> 0%
where the time goes in v1:
time: 349 us; the launch traced here: 348 us
  Pallas kernels  345 us (99%)
    pallas_call x1, Pallas kernels, on_device(): pl.pallas_call(functools.partial(kernel, n_fs, n_tp), out_shape=jax.Shape...  345 us

profile of v1, /device:TPU:0, one launch (start us, length us, event | category | flops | bytes accessed | tf_op | source)
XLA Modules:
  0.0 348.2 jit_solution(16697309380642689227)
XLA Ops:
  0.0 0.8 copy.16
  0.8 0.6 reshape.3.ffn_taps
  1.4 344.7 %shard_map.136 = bf16[768,512]{1,0:T(8,128)(2,1)} custom-call(bf16[768,512]{1,0:T(8,128)(2,1)} %tok_in.1, bf16[256,512]{1,0:T(8,128)(2,1)} %og.1, bf16[256,512]{1,0:T(8,128)(2,1)} %ig.1, bf16[256,512]{1,0:T(8,128)(2,1)} %si.1, bf16[512,256]{1,0:T(8,128)(2,1)} %mo.1, bf16[256,1408]{1,0:T(8,128)(2,1)} %ug.1, bf16[256,1408]{1,0:T(8,128)(2,1)} %uv.1, ...), custom_call_target="tpu_custom_call" | custom-call | tf_op jit(solution)/shard_map/pallas_call | solution.py:392
  346.1 2.1 copy.18
